TPU v7x, 256 devices: a whole 4x4x8 slice. The times are simulated.
256 devices in a mesh: ep: 64 (over z, x, core), tp: 4 (over y).
Axes of the slice: x: 4, y: 4, z: 8, core: 2. Of those that a mesh axis runs over, the one named last changes fastest.
Arguments:
- mix_in: bfloat16 [32768, 2048], P('ep'), may hold values from -6 to 6
- forget_shift: float32 [32768], P('ep'), may hold values from -2.5 to 2.5, as said below
- mix_gain: float32 [2048], replicated, may hold values from 0.1 to 1.9
- w_query: bfloat16 [2048, 1024], P(None, 'tp'), may hold values from -0.125 to 0.125
- w_forget: bfloat16 [2048, 1024], P(None, 'tp'), may hold values from -0.125 to 0.125
- w_value: bfloat16 [2048, 1024], P(None, 'tp'), may hold values from -0.125 to 0.125
- forget_room: float32 [1024], P('tp'), may hold values from 0 to 1, as said below
- head_gain: float32 [1024], P('tp'), may hold values from 0.1 to 1.9
- w_out: bfloat16 [1024, 2048], P('tp'), may hold values from -0.1875 to 0.1875
- moe_in: bfloat16 [16384, 2048], P('ep'), may hold values from -6 to 6
- moe_gain: float32 [2048], replicated, may hold values from 0.1 to 1.9
- expert_choice: int32 [16384, 4], P('ep'), may hold values from 0 to 63, as said below
- route_logit: float32 [16384, 4], P(('ep', 'tp')), may hold values from -6 to 6
- w_exp_gate: bfloat16 [64, 2048, 1024], P('ep', None, 'tp'), may hold values from -0.125 to 0.125
- w_exp_up: bfloat16 [64, 2048, 1024], P('ep', None, 'tp'), may hold values from -0.125 to 0.125
- w_exp_down: bfloat16 [64, 1024, 2048], P('ep', 'tp'), may hold values from -0.1875 to 0.1875
- w_sh_gate: bfloat16 [2048, 512], P(None, 'tp'), may hold values from -0.125 to 0.125
- w_sh_up: bfloat16 [2048, 512], P(None, 'tp'), may hold values from -0.125 to 0.125
- w_sh_down: bfloat16 [512, 2048], P('tp'), may hold values from -0.25 to 0.25
Outputs:
- mixer_out: bfloat16 [32768, 2048], P(('ep', 'tp'))
- moe_out: bfloat16 [16384, 2048], P(('ep', 'tp'))
Inputs may be any that keep to these rules, and one draw needn't show every extreme that they name: `forget_room`: positive and at most 1/6 in every entry. `forget_shift`: constant over each aligned span of 64 positions. `expert_choice`: each row names 4 different experts. In each aligned block of 64 rows no expert is named by more than 6 rows; in every draw one expert is named by exactly 6 rows in every block.
All inputs are finite; a program needn't handle non-finite values.
Results may differ from a plain program's by a relative error of at most 0.02.
Values may be sent and summed in bfloat16 or wider, within the bound.
No kernel may reach another device: no remote copies, remote signals or barrier semaphores. Data moves between devices by JAX's collectives and lax.ppermute only.
A program may use at most 128 MiB of HBM per device.

v0:
```python
import jax
import jax.numpy as jnp
from jax import lax
from jax.sharding import Mesh
from jax.sharding import PartitionSpec as P

HEAD_K = 64
HEAD_V = 64
SPAN = 64
TOP_K = 4
EP = ("ep_0", "ep_1", "ep_2")
EP_TP = ("ep_0", "ep_1", "ep_2", "tp")
epsilon = 1e-06
route_scale = 2.5


def neutral_like(x, identity):
    return jax.tree.map(
        lambda a, e: jnp.broadcast_to(jnp.asarray(e, a.dtype), a.shape), x, identity
    )


def prefix_by_axis(x, axes, combine, identity):
    before = start = neutral_like(x, identity)
    running = x
    for axis in reversed(axes):
        peers, index = (lax.axis_size(axis), lax.axis_index(axis))
        pieces = jax.tree.map(
            lambda part, kind: lax.all_gather(part.astype(kind), axis),
            running,
            (jnp.bfloat16, jnp.bfloat16),
        )
        inside, running = (start, start)
        for k in range(peers):
            passed = k < index
            running = combine(
                running, jax.tree.map(lambda part, own: part[k].astype(own.dtype), pieces, x)
            )
            inside = jax.tree.map(lambda new, old: jnp.where(passed, new, old), running, inside)
        before = combine(inside, before)
    return before


def norm_rows(row_data, gain_vec):
    widened = row_data.astype(jnp.float32)
    scaled = widened * lax.rsqrt(jnp.mean(widened * widened, axis=-1, keepdims=True) + epsilon)
    return (scaled * gain_vec).astype(jnp.bfloat16)


def join_states(earlier, latter):
    return (earlier[0] * latter[0], latter[0][..., None] * earlier[1] + latter[1])


def block_terms(queries, keyed, log_forget, values, span_len):
    token_count, head_count, key_width = queries.shape
    blocks = token_count // span_len
    key_shape = (blocks, span_len, head_count, key_width)
    queries = queries.reshape(key_shape)
    keyed = keyed.reshape(key_shape)
    log_forget = log_forget.reshape(key_shape)
    values = values.reshape(blocks, span_len, head_count, values.shape[-1])
    log_decay = jnp.cumsum(log_forget, axis=1)
    middle = log_decay[:, span_len // 2 : span_len // 2 + 1]
    block_end = log_decay[:, span_len - 1 :]
    scores = jnp.einsum(
        "nthd,nshd->nhts",
        queries * jnp.exp(log_decay - middle),
        keyed * jnp.exp(middle - log_decay),
    )
    causal = jnp.arange(span_len)[:, None] >= jnp.arange(span_len)[None, :]
    scores = jnp.where(causal, scores, 0.0)
    within = jnp.einsum("nhts,nshv->nthv", scores, values)
    query_decay = queries * jnp.exp(log_decay)
    decay_total = jnp.exp(block_end[:, 0])
    state_added = jnp.einsum("nshd,nshv->nhdv", keyed * jnp.exp(block_end - log_decay), values)
    return (within, query_decay, decay_total, state_added)


def local(
    mix_in,
    forget_shift,
    mix_gain,
    w_query,
    w_forget,
    w_value,
    forget_room,
    head_gain,
    w_out,
    moe_in,
    moe_gain,
    expert_choice,
    route_logit,
    w_exp_gate,
    w_exp_up,
    w_exp_down,
    w_sh_gate,
    w_sh_up,
    w_sh_down,
):
    tp_count = lax.axis_size("tp")
    tp_rank = lax.axis_index("tp")
    gate_whole, up_whole, down_whole = (
        lax.all_gather(w_exp_gate, "tp", axis=2, tiled=True),
        lax.all_gather(w_exp_up, "tp", axis=2, tiled=True),
        lax.all_gather(w_exp_down, "tp", axis=1, tiled=True),
    )
    normed = norm_rows(mix_in, mix_gain)
    queries = jax.nn.silu(jnp.dot(normed, w_query, preferred_element_type=jnp.float32))
    before = jnp.dot(normed, w_forget, preferred_element_type=jnp.float32) + forget_shift[:, None]
    values = jnp.dot(normed, w_value, preferred_element_type=jnp.float32)
    forget_rate = forget_room * jax.nn.sigmoid(-before)
    log_forget = jnp.log1p(-forget_rate)
    token_count = normed.shape[0]
    head_count = values.shape[1] // HEAD_V
    key_shape = (token_count, head_count, HEAD_K)
    within, query_decay, decay_total, state_added = block_terms(
        queries.reshape(key_shape),
        forget_rate.reshape(key_shape),
        log_forget.reshape(key_shape),
        values.reshape(token_count, head_count, HEAD_V),
        SPAN,
    )
    run_total, run_added = lax.associative_scan(join_states, (decay_total, state_added), axis=0)
    start_total, start_added = prefix_by_axis(
        (run_total[-1], run_added[-1]),
        EP,
        join_states,
        (jnp.ones_like(run_total[-1]), jnp.zeros_like(run_added[-1])),
    )
    prior_total = jnp.concatenate([jnp.ones_like(run_total[:1]), run_total[:-1]], axis=0)
    prior_added = jnp.concatenate([jnp.zeros_like(run_added[:1]), run_added[:-1]], axis=0)
    state_in = prior_total[..., None] * start_added[None] + prior_added
    mixed = within + jnp.einsum("nthd,nhdv->nthv", query_decay, state_in)
    mixed = mixed.reshape(token_count, head_count, HEAD_V)
    normal = mixed * lax.rsqrt(jnp.mean(mixed * mixed, axis=-1, keepdims=True) + epsilon)
    head_out = (normal * head_gain.reshape(head_count, HEAD_V)).astype(jnp.bfloat16)
    mixer_part = jnp.dot(
        head_out.reshape(token_count, head_count * HEAD_V),
        w_out,
        preferred_element_type=jnp.float32,
    )
    row_count = moe_in.shape[0]
    model_width = moe_in.shape[1]
    quarter = row_count // tp_count
    experts = lax.axis_size(EP) * w_exp_gate.shape[0]
    mean_load = quarter * TOP_K // experts
    capacity = mean_load + mean_load // 2
    hidden = norm_rows(moe_in, moe_gain)
    labels = expert_choice.reshape(tp_count, quarter * TOP_K)
    onehot = (labels[..., None] == jnp.arange(experts, dtype=jnp.int32)).astype(jnp.int32)
    places = jnp.sum(jnp.cumsum(onehot, axis=1) * onehot, axis=-1) - 1
    slot_ids = labels * capacity + places
    own_slots = lax.dynamic_index_in_dim(slot_ids, tp_rank, 0, keepdims=False)
    padded = jnp.concatenate([hidden, jnp.zeros((1, model_width), jnp.bfloat16)], axis=0)
    own_tokens = tp_rank * quarter + jnp.arange(quarter * TOP_K) // TOP_K
    own_source = jnp.full((experts * capacity,), row_count, jnp.int32).at[own_slots].set(own_tokens)
    outgoing = padded[own_source].reshape(1, experts, capacity, model_width)
    group_width = gate_whole.shape[2] // tp_count
    down_groups = down_whole[0].reshape(tp_count, group_width, model_width)
    arrived = lax.all_to_all(outgoing, EP, split_axis=1, concat_axis=1, tiled=True)
    gate_pre = jnp.einsum(
        "qecd,df->qecf", arrived, gate_whole[0], preferred_element_type=jnp.float32
    )
    up_pre = jnp.einsum("qecd,df->qecf", arrived, up_whole[0], preferred_element_type=jnp.float32)
    activations = (jax.nn.silu(gate_pre) * up_pre).astype(jnp.bfloat16)
    grouped = activations.reshape(activations.shape[:3] + (tp_count, group_width))
    partial_value = jnp.einsum(
        "qecgf,gfd->qecgd", grouped, down_groups, preferred_element_type=jnp.float32
    )
    summed = jnp.sum(partial_value.astype(jnp.bfloat16).astype(jnp.float32), axis=3)
    results = lax.all_to_all(
        summed.astype(jnp.bfloat16), EP, split_axis=1, concat_axis=1, tiled=True
    )
    returned_rows = results.reshape(experts * capacity, model_width)
    picked = returned_rows[own_slots].reshape(quarter, TOP_K, model_width).astype(jnp.float32)
    chance = jax.nn.sigmoid(route_logit)
    weights = chance / jnp.sum(chance, axis=-1, keepdims=True) * route_scale
    routed = jnp.sum(weights[..., None] * picked, axis=1)
    shared_gate = jnp.dot(hidden, w_sh_gate, preferred_element_type=jnp.float32)
    shared_up = jnp.dot(hidden, w_sh_up, preferred_element_type=jnp.float32)
    shared_act = (jax.nn.silu(shared_gate) * shared_up).astype(jnp.bfloat16)
    shared_part = jnp.dot(shared_act, w_sh_down, preferred_element_type=jnp.float32)
    mixer_sum, shared_sum = (
        lax.psum_scatter(
            mixer_part.astype(jnp.bfloat16), "tp", scatter_dimension=0, tiled=True
        ).astype(jnp.float32),
        lax.psum_scatter(
            shared_part.astype(jnp.bfloat16), "tp", scatter_dimension=0, tiled=True
        ).astype(jnp.float32),
    )
    return (mixer_sum.astype(jnp.bfloat16), (routed + shared_sum).astype(jnp.bfloat16))


def solution(mesh):
    finer = Mesh(mesh.devices.reshape(8, 4, 2, mesh.shape["tp"]), ("ep_0", "ep_1", "ep_2", "tp"))
    in_specs = (
        P(EP, None),
        P(EP),
        P(),
        P(None, "tp"),
        P(None, "tp"),
        P(None, "tp"),
        P("tp"),
        P("tp"),
        P("tp", None),
        P(EP, None),
        P(),
        P(EP, None),
        P(EP_TP, None),
        P(EP, None, "tp"),
        P(EP, None, "tp"),
        P(EP, "tp", None),
        P(None, "tp"),
        P(None, "tp"),
        P("tp", None),
    )
    out_specs = (P(EP_TP, None), P(EP_TP, None))
    return jax.shard_map(local, mesh=finer, in_specs=in_specs, out_specs=out_specs, check_vma=False)
```

profile of v0, /device:TPU:2, one launch (start us, length us, event | category | flops | bytes accessed | tf_op | source)
XLA Modules:
  0.0 262.9 jit_solution(2775184898795424189)
XLA Ops:
  9.9 2.4 reduce-window.6
  14.9 3.1 %gather_fusion = bf16[384,2048]{1,0:T(8,128)(2,1)} fusion(bf16[257,2048]{1,0:T(8,128)(2,1)S(1)} %concatenate.27, s32[1024]{0:T(1024)S(1)} %pad_clamp_fusion.1), kind=kCustom, calls=%fused_computation | custom fusion | bytes 3147264 | tf_op jit(solution)/shard_map/gather | solution.py:157
  18.1 3.7 %reshape.273 = bf16[1,64,6,2048]{3,2,1,0:T(8,128)(2,1)} reshape(bf16[384,2048]{1,0:T(8,128)(2,1)} %gather_fusion) | data formatting | bytes 3145728 | tf_op jit(solution)/shard_map/reshape | solution.py:157
  21.7 12.3 %all-to-all-start = ((bf16[1,64,6,2048]{3,2,0,1:T(8,128)(2,1)}), bf16[1,64,6,2048]{3,2,0,1:T(8,128)(2,1)}, u32[]{:S(2)}, u32[]{:S(2)}) async-start(bf16[1,64,6,2048]{3,2,0,1:T(8,128)(2,1)} %bitcast.171), calls=%async_computation.1 | async-start | bytes 4194304 | tf_op jit(solution)/shard_map/all_to_all | solution.py:160
  37.5 2.2 fusion
  39.9 1.9 negate_log-plus-one_fusion
  41.8 2.6 reshape_reshape.14
  47.4 2.0 all_gather.33
  51.8 2.6 %divide_multiply_fusion = f32[512,256]{1,0:T(8,128)S(1)} fusion(bf16[2048,256]{1,0:T(8,128)(2,1)} %param.22, bf16[512,2048]{1,0:T(8,128)(2,1)} %param.19, f32[2048]{0:T(1024)S(1)} %copy-done.30, f32[512]{0:T(512)S(1)} %add_rsqrt_fusion), kind=kOutput, calls=%fused_computation.66 | convolution fusion | flops 541589504 | bytes 3680256 | tf_op jit(solution)/shard_map/dot_general | solution.py:108
  56.0 2.7 %fusion.99 = bf16[512,256]{1,0:T(8,128)(2,1)S(1)} fusion(bf16[2048,256]{1,0:T(8,128)(2,1)} %param.24, bf16[512,2048]{1,0:T(8,128)(2,1)} %param.19, f32[2048]{0:T(1024)S(1)} %copy-done.30, f32[512]{0:T(512)S(1)} %add_rsqrt_fusion), kind=kOutput, calls=%fused_computation.183 | convolution fusion | flops 541065216 | bytes 3418112 | tf_op jit(solution)/shard_map/dot_general | solution.py:110
  58.9 4.2 %exponential_multiply_fusion = (bf16[8,64,4,64]{3,0,1,2:T(8,128)(2,1)}, bf16[8,64,4,64]{3,0,1,2:T(8,128)(2,1)}, bf16[8,64,4,64]{3,0,1,2:T(8,128)(2,1)}, bf16[8,64,4,64]{3,0,1,2:T(8,128)(2,1)S(1)}) fusion(f32[8,64,4,64]{3,0,1,2:T(8,128)S(1)} %fusion.32, f32[8,64,4,64]{3,2,1,0:T(4,128)} %reshape_reshape.13, f32[8,4,64]{2,0,1:T(8,128)S(1)} %get-tuple-element.11, ...), kind=kLoop, calls=%fused_computation.45 | loop fusion | flops 1441792 | bytes 2637824 | tf_op jit(solution)/shard_map/mul | solution.py:73
  64.8 3.1 %pad.49 = f32[4,4,64,64]{3,2,1,0:T(8,128)S(1)} pad(f32[2,4,64,64]{3,2,1,0:T(8,128)} %pad_maximum_fusion.1, f32[]{:T(128)} %constant.32.clone.1), padding=0_1_1x0_0_0x0_0_0x0_0_0 | pad | bytes 393220 | tf_op jit(solution)/shard_map/pad | solution.py:123
  67.9 3.2 %pad.50 = f32[4,4,64,64]{3,2,1,0:T(8,128)} pad(f32[2,4,64,64]{3,2,1,0:T(8,128)S(1)} %pad_add_fusion, f32[]{:T(128)} %constant.32.clone.1), padding=1_0_1x0_0_0x0_0_0x0_0_0 | pad | bytes 393220 | tf_op jit(solution)/shard_map/pad | solution.py:123
  73.0 9.2 %pad.101 = f32[8,4,64,64]{3,2,1,0:T(8,128)} pad(f32[4,4,64,64]{3,2,1,0:T(8,128)} %add.256, f32[]{:T(128)} %constant.32.clone.1), padding=1_0_1x0_0_0x0_0_0x0_0_0 | pad | bytes 786436
  84.7 1.9 all_gather.36
  86.6 7.8 %all_gather.34 = bf16[4,4,64]{2,1,0:T(4,128)(2,1)S(1)} all-gather(bf16[1,4,64]{2,1,0:T(4,128)(2,1)S(1)} %copy-done.27), channel_id=1, replica_groups=mesh['ep_0'=8,'ep_1'=4,'ep_2'=2,'tp'=4] {'ep_1'}, dimensions={0}, use_global_device_ids=true | all-gather | bytes 2560 | tf_op jit(solution)/shard_map/all_gather | solution.py:29
  95.7 17.1 %all_gather.35 = bf16[8,4,64]{2,1,0:T(4,128)(2,1)} all-gather(bf16[1,4,64]{2,1,0:T(4,128)(2,1)S(1)} %fusion.78), channel_id=1, replica_groups=mesh['ep_0'=8,'ep_1'=4,'ep_2'=2,'tp'=4] {'ep_0'}, dimensions={0}, use_global_device_ids=true | all-gather | bytes 4608 | tf_op jit(solution)/shard_map/all_gather | solution.py:29
  112.7 11.6 %all_gather.37 = bf16[4,4,64,64]{3,2,1,0:T(8,128)(2,1)S(1)} all-gather(bf16[1,4,64,64]{3,2,1,0:T(8,128)(2,1)S(1)} %fusion.60), channel_id=1, replica_groups=mesh['ep_0'=8,'ep_1'=4,'ep_2'=2,'tp'=4] {'ep_1'}, dimensions={0}, use_global_device_ids=true | all-gather | bytes 163840 | tf_op jit(solution)/shard_map/all_gather | solution.py:29
  125.2 27.5 %all_gather.38 = bf16[8,4,64,64]{3,2,1,0:T(8,128)(2,1)} all-gather(bf16[1,4,64,64]{3,2,1,0:T(8,128)(2,1)S(1)} %fusion.59), channel_id=1, replica_groups=mesh['ep_0'=8,'ep_1'=4,'ep_2'=2,'tp'=4] {'ep_0'}, dimensions={0}, use_global_device_ids=true | all-gather | bytes 294912 | tf_op jit(solution)/shard_map/all_gather | solution.py:29
  153.0 2.3 add_bitcast_fusion.1
  155.3 1.9 fusion.17
  161.0 2.1 convolution_convert_fusion
  163.1 5.1 %fusion.5 = f32[64,6,1024]{2,0,1:T(8,128)S(1)} fusion(bf16[1,2048,1024]{2,1,0:T(8,128)(2,1)} %all-gather.4.cloned.1.call-done, bf16[1,64,6,2048]{3,2,0,1:T(8,128)(2,1)} %all-to-all-done), kind=kOutput, calls=%fused_computation.11 | convolution fusion | flops 1610612736 | bytes 7340032 | tf_op jit(solution)/shard_map/qecd,df->qecf/dot_general | solution.py:161
  168.3 5.1 %multiply_convert_fusion = bf16[64,6,1024]{2,0,1:T(8,128)(2,1)S(1)} fusion(f32[64,6,1024]{2,0,1:T(8,128)S(1)} %fusion.5, bf16[1,2048,1024]{2,1,0:T(8,128)(2,1)} %all-gather.6.cloned.1.call-done, bf16[1,64,6,2048]{3,2,0,1:T(8,128)(2,1)} %all-to-all-done), kind=kOutput, calls=%fused_computation.23 | convolution fusion | flops 1612972032 | bytes 8126464 | tf_op jit(solution)/shard_map/qecd,df->qecf/dot_general | solution.py:164
  173.4 3.6 %all-gather.8.cloned.1.call-done = bf16[1,1024,2048]{2,1,0:T(8,128)(2,1)} async-done(((bf16[1,256,2048]{2,1,0:T(8,128)(2,1)}), bf16[1,1024,2048]{2,1,0:T(8,128)(2,1)}) %all-gather.8.cloned.1.call-update) | async-done | bytes 4194320 | tf_op jit(solution)/shard_map/all_gather | solution.py:105
  177.1 4.1 %convert_reduce_fusion = bf16[64,6,2048]{2,0,1:T(8,128)(2,1)S(1)} fusion(bf16[4,256,2048,1]{2,1,3,0:T(8,128)(2,1)} %bitcast.177, bf16[6,8,4,8,256]{4,3,2,1,0:T(8,128)(2,1)S(1)} %bitcast.178), kind=kOutput, calls=%fused_computation.3 | convolution fusion | flops 1616117760 | bytes 6553600 | tf_op jit(solution)/shard_map/qecgf,gfd->qecgd/dot_general | solution.py:167
  181.2 2.2 copy.149
  183.4 10.9 %all-to-all-start.1 = ((bf16[1,64,6,2048]{3,2,0,1:T(8,128)(2,1)}), bf16[1,64,6,2048]{3,2,0,1:T(8,128)(2,1)}, u32[]{:S(2)}, u32[]{:S(2)}) async-start(bf16[1,64,6,2048]{3,2,0,1:T(8,128)(2,1)} %copy.149), calls=%async_computation.2 | async-start | bytes 4194304 | tf_op jit(solution)/shard_map/all_to_all | solution.py:171
  194.5 51.0 %all-to-all-done.1 = bf16[1,64,6,2048]{3,2,0,1:T(8,128)(2,1)} async-done(((bf16[1,64,6,2048]{3,2,0,1:T(8,128)(2,1)}), bf16[1,64,6,2048]{3,2,0,1:T(8,128)(2,1)}, u32[]{:S(2)}, u32[]{:S(2)}) %all-to-all-start.1) | async-done | bytes 1572896 | tf_op jit(solution)/shard_map/all_to_all | solution.py:171
  245.4 2.6 reshape.276
  248.0 2.4 gather_fusion.1
  252.1 2.3 multiply_reduce_fusion
  (175 shorter events, 31.5 us)
Async XLA Ops:
  7.2 153.8 %copy-start = (bf16[256,2048]{1,0:T(8,128)(2,1)S(1)}, bf16[256,2048]{1,0:T(8,128)(2,1)}, u32[]{:S(2)}) copy-start(bf16[256,2048]{1,0:T(8,128)(2,1)} %param.27) | copy-start | bytes 3145732
  7.2 155.9 %all-gather.4.cloned.1.call-start = ((), (), s32[]{:S(2)}) async-start(), calls=%async_computation.5 | async-start | bytes 5242880 | tf_op jit(solution)/shard_map/all_gather | solution.py:103
  7.9 4.6 %copy-start.1 = (bf16[256,2048]{1,0:T(8,128)(2,1)S(1)}, bf16[256,2048]{1,0:T(8,128)(2,1)}, u32[]{:S(2)}) copy-start(bf16[256,2048]{1,0:T(8,128)(2,1)} %param.28) | copy-start | bytes 3145732
  7.9 160.4 %all-gather.6.cloned.1.call-start = ((), (), s32[]{:S(2)}) async-start(), calls=%async_computation.6 | async-start | bytes 5242880 | tf_op jit(solution)/shard_map/all_gather | solution.py:104
  8.7 4.2 %copy-start.20 = (f32[2048]{0:T(1024)S(1)}, f32[2048]{0:T(1024)}, u32[]{:S(2)}) copy-start(f32[2048]{0:T(1024)} %param.29) | copy-start | bytes 24580
  8.7 168.4 %all-gather.8.cloned.1.call-start = ((), (), s32[]{:S(2)}) async-start(), calls=%async_computation.7 | async-start | bytes 5242880 | tf_op jit(solution)/shard_map/all_gather | solution.py:105
  13.5 4.6 %copy-start.25 = (s32[256,1]{0,1:T(1,128)}, s32[256,1]{0,1:T(1,128)S(1)}, u32[]{:S(2)}) copy-start(s32[256,1]{0,1:T(1,128)S(1)} %compare_select_fusion) | copy-start | bytes 3076
  21.7 13.9 %copy-start.4 = (bf16[128,2048]{1,0:T(8,128)(2,1)S(1)}, bf16[128,2048]{1,0:T(8,128)(2,1)}, u32[]{:S(2)}) copy-start(bf16[128,2048]{1,0:T(8,128)(2,1)} %param.37) | copy-start | bytes 1572868
  21.7 13.9 %copy-start.5 = (bf16[2048,128]{1,0:T(8,128)(2,1)S(1)}, bf16[2048,128]{1,0:T(8,128)(2,1)}, u32[]{:S(2)}) copy-start(bf16[2048,128]{1,0:T(8,128)(2,1)} %param.36) | copy-start | bytes 1572868
  21.7 141.3 %all-to-all-start = ((bf16[1,64,6,2048]{3,2,0,1:T(8,128)(2,1)}), bf16[1,64,6,2048]{3,2,0,1:T(8,128)(2,1)}, u32[]{:S(2)}, u32[]{:S(2)}) async-start(bf16[1,64,6,2048]{3,2,0,1:T(8,128)(2,1)} %bitcast.171), calls=%async_computation.1 | async-start | bytes 4194304 | tf_op jit(solution)/shard_map/all_to_all | solution.py:160
  34.1 220.4 %reduce-scatter.5.cloned.1.call-start = ((), (), s32[]{:S(2)}) async-start(), calls=%async_computation.8 | async-start | bytes 1310720 | tf_op jit(solution)/shard_map/reduce_scatter | solution.py:187
  35.6 4.1 %copy-start.31 = (f32[512]{0:T(512)S(1)}, f32[512]{0:T(512)}, u32[]{:S(2)}) copy-start(f32[512]{0:T(512)} %param.20) | copy-start | bytes 6148
  37.5 218.9 %reduce-scatter.3.cloned.1.call-start = ((), (), s32[]{:S(2)}) async-start(), calls=%async_computation.4 | async-start | bytes 2621440 | tf_op jit(solution)/shard_map/reduce_scatter | solution.py:184
  41.8 8.6 %copy-start.6 = (f32[512,256]{1,0:T(8,128)S(1)}, f32[512,256]{1,0:T(8,128)}, u32[]{:S(2)}) copy-start(f32[512,256]{1,0:T(8,128)} %get-tuple-element.35) | copy-start | bytes 1572868
  45.8 8.7 %copy-start.8 = (f32[8,4,64]{2,0,1:T(8,128)}, f32[8,4,64]{2,0,1:T(8,128)S(1)}, u32[]{:S(2)}) copy-start(f32[8,4,64]{2,0,1:T(8,128)S(1)} %fusion.95) | copy-start | bytes 24580
  46.1 8.4 %copy-start.9 = (f32[4,4,64]{2,0,1:T(4,128)}, f32[4,4,64]{2,0,1:T(4,128)S(1)}, u32[]{:S(2)}) copy-start(f32[4,4,64]{2,0,1:T(4,128)S(1)} %add.249) | copy-start | bytes 12292
  49.3 5.2 %copy-start.13 = (bf16[2,4,64]{2,1,0:T(4,128)(2,1)}, bf16[2,4,64]{2,1,0:T(4,128)(2,1)S(1)}, u32[]{:S(2)}) copy-start(bf16[2,4,64]{2,1,0:T(4,128)(2,1)S(1)} %all_gather.33) | copy-start | bytes 3076
  67.9 14.3 %copy-start.15 = (f32[3,4,64]{2,1,0:T(4,128)S(1)}, f32[3,4,64]{2,1,0:T(4,128)}, u32[]{:S(2)}) copy-start(f32[3,4,64]{2,1,0:T(4,128)} %copy.132) | copy-start | bytes 9220
  82.2 4.4 %copy-start.27 = (bf16[1,4,64]{2,1,0:T(4,128)(2,1)S(1)}, bf16[1,4,64]{2,1,0:T(4,128)(2,1)}, u32[]{:S(2)}) copy-start(bf16[1,4,64]{2,1,0:T(4,128)(2,1)} %fusion.73) | copy-start | bytes 1540
  82.2 12.2 %copy-start.14 = (bf16[2,4,64]{2,1,0:T(4,128)(2,1)S(1)}, bf16[2,4,64]{2,1,0:T(4,128)(2,1)}, u32[]{:S(2)}) copy-start(bf16[2,4,64]{2,1,0:T(4,128)(2,1)} %copy-done.13) | copy-start | bytes 3076
  82.2 12.8 %copy-start.19 = (f32[4,64]{1,0:T(4,128)S(1)}, f32[4,64]{1,0:T(4,128)}, u32[]{:S(2)}) copy-start(f32[4,64]{1,0:T(4,128)} %convert_bitcast_fusion.4) | copy-start | bytes 3076
  82.2 13.4 %slice-start = ((f32[8,4,64]{2,0,1:T(8,128)}), f32[1,4,64]{2,0,1:T(1,128)S(1)}, s32[]{:S(2)}) async-start(f32[8,4,64]{2,0,1:T(8,128)} %copy-done.8), calls=%async_computation.9 | async-start | bytes 4096 | tf_op jit(solution)/shard_map/slice | solution.py:123
  82.2 13.3 %copy-start.11 = (f32[3,4,64]{2,0,1:T(4,128)S(1)}, f32[3,4,64]{2,0,1:T(4,128)}, u32[]{:S(2)}) copy-start(f32[3,4,64]{2,0,1:T(4,128)} %add_multiply_fusion.1) | copy-start | bytes 9220
  82.2 13.4 %copy-start.10 = (f32[4,4,64]{2,0,1:T(4,128)S(1)}, f32[4,4,64]{2,0,1:T(4,128)}, u32[]{:S(2)}) copy-start(f32[4,4,64]{2,0,1:T(4,128)} %copy-done.9) | copy-start | bytes 12292
  95.0 30.2 %copy-start.16 = (f32[4,64]{1,0:T(4,128)}, f32[4,64]{1,0:T(4,128)S(1)}, u32[]{:S(2)}) copy-start(f32[4,64]{1,0:T(4,128)S(1)} %get-tuple-element.26) | copy-start | bytes 3076
  124.4 28.6 %copy-start.12 = (bf16[8,4,64]{2,1,0:T(4,128)(2,1)S(1)}, bf16[8,4,64]{2,1,0:T(4,128)(2,1)}, u32[]{:S(2)}) copy-start(bf16[8,4,64]{2,1,0:T(4,128)(2,1)} %all_gather.35) | copy-start | bytes 12292
  124.4 28.6 %copy-start.18 = (f32[4,64]{1,0:T(4,128)S(1)}, f32[4,64]{1,0:T(4,128)}, u32[]{:S(2)}) copy-start(f32[4,64]{1,0:T(4,128)} %copy-done.17) | copy-start | bytes 3076
  124.4 28.6 %copy-start.21 = (f32[4,64]{1,0:T(4,128)S(1)}, f32[4,64]{1,0:T(4,128)}, u32[]{:S(2)}) copy-start(f32[4,64]{1,0:T(4,128)} %get-tuple-element.2) | copy-start | bytes 3076
  124.4 28.6 %copy-start.22 = (f32[4,64]{1,0:T(4,128)S(1)}, f32[4,64]{1,0:T(4,128)}, u32[]{:S(2)}) copy-start(f32[4,64]{1,0:T(4,128)} %get-tuple-element.3) | copy-start | bytes 3076
  183.4 10.9 %copy-start.23 = (f32[64,4]{0,1:T(4,128)S(1)}, f32[64,4]{0,1:T(4,128)}, u32[]{:S(2)}) copy-start(f32[64,4]{0,1:T(4,128)} %param.31) | copy-start | bytes 3076
  183.4 11.0 %copy-start.26 = (s32[256,1]{0,1:T(1,128)S(1)}, s32[256,1]{0,1:T(1,128)}, u32[]{:S(2)}) copy-start(s32[256,1]{0,1:T(1,128)} %copy-done.25) | copy-start | bytes 3076
  183.4 62.0 %all-to-all-start.1 = ((bf16[1,64,6,2048]{3,2,0,1:T(8,128)(2,1)}), bf16[1,64,6,2048]{3,2,0,1:T(8,128)(2,1)}, u32[]{:S(2)}, u32[]{:S(2)}) async-start(bf16[1,64,6,2048]{3,2,0,1:T(8,128)(2,1)} %copy.149), calls=%async_computation.2 | async-start | bytes 4194304 | tf_op jit(solution)/shard_map/all_to_all | solution.py:171
  (9 other events, 16.1 us)
Sparse Core Ops, SparseCore 0:
  9.8 56.9 all-gather.3
  68.6 54.8 all-gather.5
  125.3 51.7 all-gather.7
  179.5 26.6 reduce-scatter.4
  209.1 32.0 reduce-scatter.2
where the time goes:
time: 265 us; the launch traced here: 263 us
  blocking collectives  67.9 us (26%)
  waiting for transfers between devices  56.7 us (21%)
  local copies, waits for them, and re-layouts  42.2 us (16%)
  matrix products  30.4 us (11%)
  other arithmetic  27.6 us (10%)
  starting transfers between devices  23.4 us (9%)
  between operations  14.6 us (6%)
    all_gather x6, blocking collectives, prefix_by_axis(): lax.all_gather(part.astype(kind), axis)  67.9 us
    all_to_all x1, waiting for transfers between devices, local(): lax.all_to_all(summed.astype(jnp.bfloat16), EP, split_axis=1, concat_axis...  51 us
    all_to_all x1, starting transfers between devices, local(): lax.all_to_all(outgoing, EP, split_axis=1, concat_axis=1, tiled=True)  12.3 us
    all_to_all x1, starting transfers between devices, local(): lax.all_to_all(summed.astype(jnp.bfloat16), EP, split_axis=1, concat_axis...  10.9 us
    unnamed x70, local copies, waits for them, and re-layouts  10.1 us
    pad x7, local copies, waits for them, and re-layouts, local(): lax.associative_scan(join_states, (decay_total, state_added), axis=0)  6.75 us
  transfers between devices with their start and end apart: 7, of which 2 were waited for; matrix products, arithmetic and copies ran while one was open for 38% of the time, Pallas kernels for 0%

commit v1 on v0

--- a/solution.py
+++ b/solution.py
@@ -157,7 +157,9 @@
     outgoing = padded[own_source].reshape(1, experts, capacity, model_width)
     group_width = gate_whole.shape[2] // tp_count
     down_groups = down_whole[0].reshape(tp_count, group_width, model_width)
-    arrived = lax.all_to_all(outgoing, EP, split_axis=1, concat_axis=1, tiled=True)
+    arrived = jnp.concatenate(
+        lax.all_to_all(jnp.stack(jnp.split(outgoing, lax.axis_size(EP), axis=1)), EP, 0, 0), axis=1
+    )
     gate_pre = jnp.einsum(
         "qecd,df->qecf", arrived, gate_whole[0], preferred_element_type=jnp.float32
     )

time: 265 us -> 351 us (1.32); the launches traced: 263 us -> 345 us
  local copies, waits for them, and re-layouts: 42.2 us -> 129 us
  waiting for transfers between devices: 56.7 us -> 53.1 us
    unnamed x70 -> x133, local copies, waits for them, and re-layouts: 10.1 us -> 95.9 us
    all_gather x1, waiting for transfers between devices: 3.63 us -> 0.02 us  [local(): lax.all_gather(w_exp_down, 'tp', axis=1, tiled=True)]
  transfers between devices with their start and end apart: 7 -> 7, of which waited for: 2 -> 1; matrix products, arithmetic and copies ran while one was open for 38% -> 54% of each run, Pallas kernels for 0% -> 0%
where the time goes in v1:
time: 351 us; the launch traced here: 345 us
  local copies, waits for them, and re-layouts  129 us (37%)
  blocking collectives  67.7 us (19%)
  waiting for transfers between devices  53.1 us (15%)
  matrix products  30.8 us (9%)
  other arithmetic  27.6 us (8%)
  starting transfers between devices  21.5 us (6%)
  between operations  14.6 us (4%)
    unnamed x133, local copies, waits for them, and re-layouts  95.9 us
    all_gather x6, blocking collectives, prefix_by_axis(): lax.all_gather(part.astype(kind), axis)  67.7 us
    all_to_all x1, waiting for transfers between devices, local(): lax.all_to_all(summed.astype(jnp.bfloat16), EP, split_axis=1, concat_axis...  51 us
    all_to_all x1, starting transfers between devices, local(): lax.all_to_all(jnp.stack(jnp.split(outgoing, lax.axis_size(EP), axis=1)),...  12.3 us
    all_to_all x1, starting transfers between devices, local(): lax.all_to_all(summed.astype(jnp.bfloat16), EP, split_axis=1, concat_axis...  8.98 us
  transfers between devices with their start and end apart: 7, of which 1 were waited for; matrix products, arithmetic and copies ran while one was open for 54% of the time, Pallas kernels for 0%

profile of v1, /device:TPU:2, one launch (start us, length us, event | category | flops | bytes accessed | tf_op | source)
XLA Modules:
  0.0 344.7 jit_solution(12743626344734556428)
XLA Ops:
  9.9 2.4 reduce-window.6
  14.9 3.1 gather_fusion
  18.1 3.7 %reshape.276 = bf16[1,64,6,2048]{3,2,1,0:T(8,128)(2,1)} reshape(bf16[384,2048]{1,0:T(8,128)(2,1)} %gather_fusion) | data formatting | bytes 3145728 | tf_op jit(solution)/shard_map/reshape | solution.py:157
  109.0 12.3 %all-to-all-start = ((bf16[64,1,1,6,2048]{4,3,2,1,0:T(8,128)(2,1)}), bf16[64,1,1,6,2048]{4,3,2,1,0:T(8,128)(2,1)}, u32[]{:S(2)}, u32[]{:S(2)}) async-start(bf16[64,1,1,6,2048]{4,3,2,1,0:T(8,128)(2,1)} %constant_dynamic-update-slice_fusion), calls=%async_computation.1 | async-start | bytes 4194304 | tf_op jit(solution)/shard_map/all_to_all | solution.py:161
  124.8 2.2 fusion
  127.2 1.9 negate_log-plus-one_fusion
  129.1 2.6 reshape_reshape.14
  134.6 2.0 all_gather.33
  139.1 2.8 divide_multiply_fusion
  143.4 2.6 fusion.99
  146.3 4.1 %exponential_multiply_fusion = (bf16[8,64,4,64]{3,0,1,2:T(8,128)(2,1)}, bf16[8,64,4,64]{3,0,1,2:T(8,128)(2,1)}, bf16[8,64,4,64]{3,0,1,2:T(8,128)(2,1)}, bf16[8,64,4,64]{3,0,1,2:T(8,128)(2,1)S(1)}) fusion(f32[8,64,4,64]{3,0,1,2:T(8,128)S(1)} %fusion.32, f32[8,64,4,64]{3,2,1,0:T(4,128)} %reshape_reshape.13, f32[8,4,64]{2,0,1:T(8,128)S(1)} %get-tuple-element.11, ...), kind=kLoop, calls=%fused_computation.45 | loop fusion | flops 1441792 | bytes 2637824 | tf_op jit(solution)/shard_map/mul | solution.py:73
  152.1 3.1 pad.49
  155.2 3.3 pad.50
  158.5 1.9 add.256
  160.4 9.2 %pad.101 = f32[8,4,64,64]{3,2,1,0:T(8,128)} pad(f32[4,4,64,64]{3,2,1,0:T(8,128)} %add.256, f32[]{:T(128)} %constant.32.clone.1), padding=1_0_1x0_0_0x0_0_0x0_0_0 | pad | bytes 786436
  172.0 1.9 all_gather.36
  173.9 7.8 %all_gather.34 = bf16[4,4,64]{2,1,0:T(4,128)(2,1)S(1)} all-gather(bf16[1,4,64]{2,1,0:T(4,128)(2,1)S(1)} %copy-done.27), channel_id=1, replica_groups=mesh['ep_0'=8,'ep_1'=4,'ep_2'=2,'tp'=4] {'ep_1'}, dimensions={0}, use_global_device_ids=true | all-gather | bytes 2560 | tf_op jit(solution)/shard_map/all_gather | solution.py:29
  183.0 16.9 %all_gather.35 = bf16[8,4,64]{2,1,0:T(4,128)(2,1)} all-gather(bf16[1,4,64]{2,1,0:T(4,128)(2,1)S(1)} %fusion.78), channel_id=1, replica_groups=mesh['ep_0'=8,'ep_1'=4,'ep_2'=2,'tp'=4] {'ep_0'}, dimensions={0}, use_global_device_ids=true | all-gather | bytes 4608 | tf_op jit(solution)/shard_map/all_gather | solution.py:29
  199.9 11.4 %all_gather.37 = bf16[4,4,64,64]{3,2,1,0:T(8,128)(2,1)S(1)} all-gather(bf16[1,4,64,64]{3,2,1,0:T(8,128)(2,1)S(1)} %fusion.60), channel_id=1, replica_groups=mesh['ep_0'=8,'ep_1'=4,'ep_2'=2,'tp'=4] {'ep_1'}, dimensions={0}, use_global_device_ids=true | all-gather | bytes 163840 | tf_op jit(solution)/shard_map/all_gather | solution.py:29
  212.1 27.7 %all_gather.38 = bf16[8,4,64,64]{3,2,1,0:T(8,128)(2,1)} all-gather(bf16[1,4,64,64]{3,2,1,0:T(8,128)(2,1)S(1)} %fusion.59), channel_id=1, replica_groups=mesh['ep_0'=8,'ep_1'=4,'ep_2'=2,'tp'=4] {'ep_0'}, dimensions={0}, use_global_device_ids=true | all-gather | bytes 294912 | tf_op jit(solution)/shard_map/all_gather | solution.py:29
  240.1 2.3 add_bitcast_fusion.1
  242.4 1.9 fusion.17
  248.1 2.1 convolution_convert_fusion
  250.2 5.1 %fusion.5 = f32[64,6,1024]{2,0,1:T(8,128)S(1)} fusion(bf16[1,2048,1024]{2,1,0:T(8,128)(2,1)} %all-gather.4.cloned.1.call-done, bf16[64,1,1,6,2048]{4,3,2,1,0:T(8,128)(2,1)} %all-to-all-done), kind=kOutput, calls=%fused_computation.11 | convolution fusion | flops 1610612736 | bytes 7340032 | tf_op jit(solution)/shard_map/qecd,df->qecf/dot_general | solution.py:163
  255.3 5.1 %multiply_convert_fusion = bf16[64,6,1024]{2,0,1:T(8,128)(2,1)S(1)} fusion(f32[64,6,1024]{2,0,1:T(8,128)S(1)} %fusion.5, bf16[1,2048,1024]{2,1,0:T(8,128)(2,1)} %all-gather.6.cloned.1.call-done, bf16[64,1,1,6,2048]{4,3,2,1,0:T(8,128)(2,1)} %all-to-all-done), kind=kOutput, calls=%fused_computation.23 | convolution fusion | flops 1612972032 | bytes 8126464 | tf_op jit(solution)/shard_map/qecd,df->qecf/dot_general | solution.py:166
  260.5 4.5 %convert_reduce_fusion = bf16[64,6,2048]{2,0,1:T(8,128)(2,1)S(1)} fusion(bf16[4,256,2048,1]{2,1,3,0:T(8,128)(2,1)} %bitcast.431, bf16[6,8,4,8,256]{4,3,2,1,0:T(8,128)(2,1)S(1)} %bitcast.432), kind=kOutput, calls=%fused_computation.3 | convolution fusion | flops 1616117760 | bytes 6553600 | tf_op jit(solution)/shard_map/qecgf,gfd->qecgd/dot_general | solution.py:169
  265.0 2.2 copy.299
  267.2 9.0 %all-to-all-start.1 = ((bf16[1,64,6,2048]{3,2,0,1:T(8,128)(2,1)}), bf16[1,64,6,2048]{3,2,0,1:T(8,128)(2,1)}, u32[]{:S(2)}, u32[]{:S(2)}) async-start(bf16[1,64,6,2048]{3,2,0,1:T(8,128)(2,1)} %copy.299), calls=%async_computation.2 | async-start | bytes 4194304 | tf_op jit(solution)/shard_map/all_to_all | solution.py:173
  276.3 51.0 %all-to-all-done.1 = bf16[1,64,6,2048]{3,2,0,1:T(8,128)(2,1)} async-done(((bf16[1,64,6,2048]{3,2,0,1:T(8,128)(2,1)}), bf16[1,64,6,2048]{3,2,0,1:T(8,128)(2,1)}, u32[]{:S(2)}, u32[]{:S(2)}) %all-to-all-start.1) | async-done | bytes 1572896 | tf_op jit(solution)/shard_map/all_to_all | solution.py:173
  327.3 2.6 reshape.279
  329.9 2.4 gather_fusion.1
  334.0 2.3 multiply_reduce_fusion
  (239 shorter events, 116.8 us)
Async XLA Ops:
  7.2 240.9 %copy-start = (bf16[256,2048]{1,0:T(8,128)(2,1)S(1)}, bf16[256,2048]{1,0:T(8,128)(2,1)}, u32[]{:S(2)}) copy-start(bf16[256,2048]{1,0:T(8,128)(2,1)} %param.27) | copy-start | bytes 3145732
  7.2 243.0 %all-gather.4.cloned.1.call-start = ((), (), s32[]{:S(2)}) async-start(), calls=%async_computation.5 | async-start | bytes 5242880 | tf_op jit(solution)/shard_map/all_gather | solution.py:103
  7.9 6.3 %copy-start.1 = (bf16[256,2048]{1,0:T(8,128)(2,1)S(1)}, bf16[256,2048]{1,0:T(8,128)(2,1)}, u32[]{:S(2)}) copy-start(bf16[256,2048]{1,0:T(8,128)(2,1)} %param.28) | copy-start | bytes 3145732
  7.9 247.3 %all-gather.6.cloned.1.call-start = ((), (), s32[]{:S(2)}) async-start(), calls=%async_computation.6 | async-start | bytes 5242880 | tf_op jit(solution)/shard_map/all_gather | solution.py:104
  8.7 5.8 %copy-start.20 = (f32[2048]{0:T(1024)S(1)}, f32[2048]{0:T(1024)}, u32[]{:S(2)}) copy-start(f32[2048]{0:T(1024)} %param.29) | copy-start | bytes 24580
  8.7 251.8 %all-gather.8.cloned.1.call-start = ((), (), s32[]{:S(2)}) async-start(), calls=%async_computation.7 | async-start | bytes 5242880 | tf_op jit(solution)/shard_map/all_gather | solution.py:105
  109.0 13.9 %copy-start.4 = (bf16[128,2048]{1,0:T(8,128)(2,1)S(1)}, bf16[128,2048]{1,0:T(8,128)(2,1)}, u32[]{:S(2)}) copy-start(bf16[128,2048]{1,0:T(8,128)(2,1)} %param.37) | copy-start | bytes 1572868
  109.0 13.9 %copy-start.5 = (bf16[2048,128]{1,0:T(8,128)(2,1)S(1)}, bf16[2048,128]{1,0:T(8,128)(2,1)}, u32[]{:S(2)}) copy-start(bf16[2048,128]{1,0:T(8,128)(2,1)} %param.36) | copy-start | bytes 1572868
  109.0 141.1 %all-to-all-start = ((bf16[64,1,1,6,2048]{4,3,2,1,0:T(8,128)(2,1)}), bf16[64,1,1,6,2048]{4,3,2,1,0:T(8,128)(2,1)}, u32[]{:S(2)}, u32[]{:S(2)}) async-start(bf16[64,1,1,6,2048]{4,3,2,1,0:T(8,128)(2,1)} %constant_dynamic-update-slice_fusion), calls=%async_computation.1 | async-start | bytes 4194304 | tf_op jit(solution)/shard_map/all_to_all | solution.py:161
  121.4 215.0 %reduce-scatter.5.cloned.1.call-start = ((), (), s32[]{:S(2)}) async-start(), calls=%async_computation.8 | async-start | bytes 1310720 | tf_op jit(solution)/shard_map/reduce_scatter | solution.py:189
  122.9 4.1 %copy-start.31 = (f32[512]{0:T(512)S(1)}, f32[512]{0:T(512)}, u32[]{:S(2)}) copy-start(f32[512]{0:T(512)} %param.20) | copy-start | bytes 6148
  124.7 213.5 %reduce-scatter.3.cloned.1.call-start = ((), (), s32[]{:S(2)}) async-start(), calls=%async_computation.4 | async-start | bytes 2621440 | tf_op jit(solution)/shard_map/reduce_scatter | solution.py:186
  124.8 2.4 copy-start.29
  129.1 8.6 %copy-start.6 = (f32[512,256]{1,0:T(8,128)S(1)}, f32[512,256]{1,0:T(8,128)}, u32[]{:S(2)}) copy-start(f32[512,256]{1,0:T(8,128)} %get-tuple-element.35) | copy-start | bytes 1572868
  133.0 8.9 %copy-start.8 = (f32[8,4,64]{2,0,1:T(8,128)}, f32[8,4,64]{2,0,1:T(8,128)S(1)}, u32[]{:S(2)}) copy-start(f32[8,4,64]{2,0,1:T(8,128)S(1)} %fusion.95) | copy-start | bytes 24580
  133.4 8.6 %copy-start.9 = (f32[4,4,64]{2,0,1:T(4,128)}, f32[4,4,64]{2,0,1:T(4,128)S(1)}, u32[]{:S(2)}) copy-start(f32[4,4,64]{2,0,1:T(4,128)S(1)} %add.249) | copy-start | bytes 12292
  136.6 5.4 %copy-start.13 = (bf16[2,4,64]{2,1,0:T(4,128)(2,1)}, bf16[2,4,64]{2,1,0:T(4,128)(2,1)S(1)}, u32[]{:S(2)}) copy-start(bf16[2,4,64]{2,1,0:T(4,128)(2,1)S(1)} %all_gather.33) | copy-start | bytes 3076
  155.2 14.4 %copy-start.15 = (f32[3,4,64]{2,1,0:T(4,128)S(1)}, f32[3,4,64]{2,1,0:T(4,128)}, u32[]{:S(2)}) copy-start(f32[3,4,64]{2,1,0:T(4,128)} %copy.283) | copy-start | bytes 9220
  169.6 4.3 %copy-start.27 = (bf16[1,4,64]{2,1,0:T(4,128)(2,1)S(1)}, bf16[1,4,64]{2,1,0:T(4,128)(2,1)}, u32[]{:S(2)}) copy-start(bf16[1,4,64]{2,1,0:T(4,128)(2,1)} %fusion.73) | copy-start | bytes 1540
  169.6 12.1 %copy-start.14 = (bf16[2,4,64]{2,1,0:T(4,128)(2,1)S(1)}, bf16[2,4,64]{2,1,0:T(4,128)(2,1)}, u32[]{:S(2)}) copy-start(bf16[2,4,64]{2,1,0:T(4,128)(2,1)} %copy-done.13) | copy-start | bytes 3076
  169.6 12.7 %copy-start.19 = (f32[4,64]{1,0:T(4,128)S(1)}, f32[4,64]{1,0:T(4,128)}, u32[]{:S(2)}) copy-start(f32[4,64]{1,0:T(4,128)} %convert_bitcast_fusion.4) | copy-start | bytes 3076
  169.6 13.3 %slice-start = ((f32[8,4,64]{2,0,1:T(8,128)}), f32[1,4,64]{2,0,1:T(1,128)S(1)}, s32[]{:S(2)}) async-start(f32[8,4,64]{2,0,1:T(8,128)} %copy-done.8), calls=%async_computation.9 | async-start | bytes 4096 | tf_op jit(solution)/shard_map/slice | solution.py:123
  169.6 13.3 %copy-start.11 = (f32[3,4,64]{2,0,1:T(4,128)S(1)}, f32[3,4,64]{2,0,1:T(4,128)}, u32[]{:S(2)}) copy-start(f32[3,4,64]{2,0,1:T(4,128)} %add_multiply_fusion.1) | copy-start | bytes 9220
  169.6 13.3 %copy-start.10 = (f32[4,4,64]{2,0,1:T(4,128)S(1)}, f32[4,4,64]{2,0,1:T(4,128)}, u32[]{:S(2)}) copy-start(f32[4,4,64]{2,0,1:T(4,128)} %copy-done.9) | copy-start | bytes 12292
  182.3 29.8 %copy-start.16 = (f32[4,64]{1,0:T(4,128)}, f32[4,64]{1,0:T(4,128)S(1)}, u32[]{:S(2)}) copy-start(f32[4,64]{1,0:T(4,128)S(1)} %get-tuple-element.26) | copy-start | bytes 3076
  211.3 28.8 %copy-start.12 = (bf16[8,4,64]{2,1,0:T(4,128)(2,1)S(1)}, bf16[8,4,64]{2,1,0:T(4,128)(2,1)}, u32[]{:S(2)}) copy-start(bf16[8,4,64]{2,1,0:T(4,128)(2,1)} %all_gather.35) | copy-start | bytes 12292
  211.3 28.8 %copy-start.18 = (f32[4,64]{1,0:T(4,128)S(1)}, f32[4,64]{1,0:T(4,128)}, u32[]{:S(2)}) copy-start(f32[4,64]{1,0:T(4,128)} %copy-done.17) | copy-start | bytes 3076
  211.3 28.8 %copy-start.21 = (f32[4,64]{1,0:T(4,128)S(1)}, f32[4,64]{1,0:T(4,128)}, u32[]{:S(2)}) copy-start(f32[4,64]{1,0:T(4,128)} %get-tuple-element.2) | copy-start | bytes 3076
  211.3 28.8 %copy-start.22 = (f32[4,64]{1,0:T(4,128)S(1)}, f32[4,64]{1,0:T(4,128)}, u32[]{:S(2)}) copy-start(f32[4,64]{1,0:T(4,128)} %get-tuple-element.3) | copy-start | bytes 3076
  267.2 9.0 %copy-start.23 = (f32[64,4]{0,1:T(4,128)S(1)}, f32[64,4]{0,1:T(4,128)}, u32[]{:S(2)}) copy-start(f32[64,4]{0,1:T(4,128)} %param.31) | copy-start | bytes 3076
  267.2 9.1 %copy-start.26 = (s32[256,1]{0,1:T(1,128)S(1)}, s32[256,1]{0,1:T(1,128)}, u32[]{:S(2)}) copy-start(s32[256,1]{0,1:T(1,128)} %copy-done.25) | copy-start | bytes 3076
  267.2 60.1 %all-to-all-start.1 = ((bf16[1,64,6,2048]{3,2,0,1:T(8,128)(2,1)}), bf16[1,64,6,2048]{3,2,0,1:T(8,128)(2,1)}, u32[]{:S(2)}, u32[]{:S(2)}) async-start(bf16[1,64,6,2048]{3,2,0,1:T(8,128)(2,1)} %copy.299), calls=%async_computation.2 | async-start | bytes 4194304 | tf_op jit(solution)/shard_map/all_to_all | solution.py:173
  (9 other events, 15.3 us)
Sparse Core Ops, SparseCore 0:
  9.8 56.9 all-gather.3
  68.6 54.8 all-gather.5
  125.3 51.7 all-gather.7
  179.5 26.6 reduce-scatter.4
  250.3 32.2 reduce-scatter.2
